TPU v7x, 32 devices: a whole 2x2x4 slice. The times are simulated.
32 devices in a mesh: sp: 8 (over z, x), tp: 4 (over y, core).
Axes of the slice: x: 2, y: 2, z: 4, core: 2. Of those that a mesh axis runs over, the one named last changes fastest.
Arguments:
- residual: bfloat16 [4096, 2048], P('sp', 'tp'), may hold values from -64 to 64
- gains: float32 [2, 2, 2048], replicated, may hold values from 0.1 to 1.9
- w_query: bfloat16 [2, 2048, 2048], P(None, None, 'tp'), may hold values from -0.125 to 0.125
- w_key: bfloat16 [2, 2048, 2048], P(None, None, 'tp'), may hold values from -0.125 to 0.125
- w_value: bfloat16 [2, 2048, 2048], P(None, None, 'tp'), may hold values from -0.125 to 0.125
- w_out: bfloat16 [2, 2048, 2048], P(None, None, 'tp'), may hold values from -1 to 1
- rel_bias: float32 [2, 32, 257], P(None, 'tp'), may hold values from -6 to 300
Outputs:
- encoded: bfloat16 [4096, 2048], P('sp', 'tp')
All inputs are finite; a program needn't handle non-finite values.
Results may differ from a plain program's by a relative error of at most 0.0058.
Values may be sent and summed in bfloat16 or wider, within the bound.
A program may use at most 128 MiB of HBM per device.

v0:
```python
import functools

import jax
import jax.numpy as jnp
from jax import lax
from jax.experimental import pallas as pl
from jax.experimental.pallas import tpu as pltpu
from jax.sharding import PartitionSpec as P

HEAD = 64
SEG = 64
LEFT = 8
MAXREL = 128
BLOCK = 128
EPS = 1e-06
LOG2E = 1.4426950408889634
NEG = -1e30
MESH = pl.DeviceIdType.MESH
F32 = jnp.float32
BF16 = jnp.bfloat16


def remote(src, dst, send_sem, recv_sem, where):
    return pltpu.make_async_remote_copy(
        src_ref=src,
        dst_ref=dst,
        send_sem=send_sem,
        recv_sem=recv_sem,
        device_id=where,
        device_id_type=MESH,
    )


def kernel(
    tp,
    sp_count,
    res_ref,
    gains_ref,
    bias_ref,
    wq_ref,
    wk_ref,
    wv_ref,
    wo_ref,
    out_ref,
    wbuf,
    gather,
    kbuf,
    vbuf,
    qbuf,
    branch,
    toeplitz,
    sums,
    w_sem,
    g_send,
    g_recv,
    f_send,
    h_send,
    h_recv,
    s_send,
    s_recv,
):
    layers = wbuf.shape[0]
    tokens, cols = res_ref.shape
    width = cols * tp
    chunks = tokens // BLOCK
    pairs = cols // 128
    reach = LEFT * SEG
    blocks = reach // BLOCK
    me = lax.axis_index("tp")
    sp = lax.axis_index("sp")
    core = lax.rem(me, 2)
    sibling = me + 1 - 2 * core
    ychips = tp // 2

    weights = (wq_ref, wk_ref, wv_ref, wo_ref)

    def weight_copy(l, k):
        return pltpu.make_async_copy(weights[k].at[l], wbuf.at[l, k], w_sem.at[l, k])

    for l in range(layers):
        for k in range(4):
            weight_copy(l, k).start()

    barrier = pltpu.get_barrier_semaphore()
    for k in range(1, tp):
        pl.semaphore_signal(
            barrier, inc=1, device_id={"tp": lax.rem(me + k, tp)}, device_id_type=MESH
        )
    for k in (1, sp_count - 1):
        pl.semaphore_signal(
            barrier, inc=1, device_id={"sp": lax.rem(sp + k, sp_count)}, device_id_type=MESH
        )
    pl.semaphore_wait(barrier, tp + 1)

    def rows_of(c):
        return pl.ds(pl.multiple_of(c * BLOCK, BLOCK), BLOCK)

    def block_of(kind, l, c, slot):
        return gather.at[kind, l, slot, rows_of(c)]

    def direct(kind, l, c, peer, source):
        ref = block_of(kind, l, c, source)
        return remote(
            ref, ref, g_send.at[kind, c, peer], g_recv.at[kind, l, c, source], {"tp": peer}
        )

    def forward(kind, l, c, source):
        ref = block_of(kind, l, c, source)
        return remote(
            ref, ref, f_send.at[source], g_recv.at[kind, l, c, source], {"tp": sibling}
        )

    def spread(kind, l, c):
        for k in range(1, ychips):
            direct(kind, l, c, lax.rem(me + 2 * k, tp), me).start()
        direct(kind, l, c, sibling, me).start()

    def arrive(kind, l, c):
        for k in range(1, ychips):
            source = lax.rem(me + 2 * k, tp)
            direct(kind, l, c, source, source).wait_recv()
            forward(kind, l, c, source).start()
        direct(kind, l, c, sibling, sibling).wait_recv()
        for k in range(1, ychips):
            source = lax.rem(sibling + 2 * k, tp)
            direct(kind, l, c, sibling, source).wait_recv()
        for k in range(1, ychips):
            forward(kind, l, c, lax.rem(me + 2 * k, tp)).wait_send()
            direct(kind, l, c, lax.rem(me + 2 * k, tp), me).wait_send()
        direct(kind, l, c, sibling, me).wait_send()

    def halo(l, c, which):
        buf = (kbuf, vbuf)[which]
        return remote(
            buf.at[l, rows_of(c + blocks)],
            buf.at[l, rows_of(c)],
            h_send.at[c, which],
            h_recv.at[l, c, which],
            {"sp": lax.rem(sp + 1, sp_count)},
        )

    def sum_copy(l, c, peer, source):
        ref = sums.at[l, c, source]
        return remote(ref, ref, s_send.at[peer], s_recv.at[l, c, source], {"tp": peer})

    gather[0, 0, me] = res_ref[...]
    for t in range(chunks):
        spread(0, 0, chunks - 1 - t)

    @pl.when(sp == 0)
    def _():
        for l in range(layers):
            kbuf[l, :reach] = jnp.zeros((reach, cols), BF16)
            vbuf[l, :reach] = jnp.zeros((reach, cols), BF16)

    row = lax.broadcasted_iota(jnp.int32, (BLOCK, BLOCK), 0)
    col = lax.broadcasted_iota(jnp.int32, (BLOCK, BLOCK), 1)
    low = col < HEAD
    early = jnp.where((row >= SEG) & (col < SEG), NEG, 0.0).astype(F32)
    late = jnp.where((row < SEG) & (col >= SEG), NEG, 0.0).astype(F32)

    def project(l, c):
        arrive(0, l, c)
        parts = [gather[0, l, j, rows_of(c)].astype(F32) for j in range(tp)]
        total = sum(jnp.sum(p * p, axis=1, keepdims=True) for p in parts)
        inv = lax.rsqrt(total / width + EPS)
        gain = gains_ref[l, 0:1, :]
        normed = jnp.concatenate(
            [
                (p * inv * gain[:, j * cols : (j + 1) * cols]).astype(BF16)
                for j, p in enumerate(parts)
            ],
            axis=1,
        )
        own = rows_of(c + blocks)
        kbuf[l, own] = jnp.dot(normed, wbuf[l, 1], preferred_element_type=F32).astype(BF16)
        vbuf[l, own] = jnp.dot(normed, wbuf[l, 2], preferred_element_type=F32).astype(BF16)

        @pl.when(sp < sp_count - 1)
        def _():
            halo(l, c, 0).start()
            halo(l, c, 1).start()

        query = jnp.dot(normed, wbuf[l, 0], preferred_element_type=F32)
        qbuf[rows_of(c)] = (query * (LOG2E * HEAD**-0.5)).astype(BF16)

    def attention(l, c):
        @pl.when(sp > 0)
        def _():
            halo(l, c, 0).wait_recv()
            halo(l, c, 1).wait_recv()

        @pl.when(sp < sp_count - 1)
        def _():
            halo(l, c, 0).wait_send()
            halo(l, c, 1).wait_send()

        window = pl.ds(pl.multiple_of(c * BLOCK, BLOCK), reach + BLOCK)
        closed = [
            jnp.where((sp == 0) & (c + i < blocks), NEG, 0.0).astype(F32) for i in range(blocks)
        ]

        for pair in range(pairs):
            lanes = slice(pair * 128, (pair + 1) * 128)
            query = qbuf[rows_of(c), lanes]
            keys = kbuf[l, window, lanes]
            values = vbuf[l, window, lanes]
            halves = []
            for half in range(2):
                mine = low if half == 0 else ~low
                masked = jnp.where(mine, query.astype(F32), 0.0).astype(BF16)
                scores = lax.dot_general(
                    masked, keys, (((1,), (1,)), ((), ())), preferred_element_type=F32
                )
                tiles = []
                for i in range(blocks + 1):
                    tile = scores[:, i * BLOCK : (i + 1) * BLOCK]
                    if i == 0:
                        tile = tile + early
                    if i >= blocks - 1:
                        at = (i - blocks + 1) * BLOCK
                        tile = tile + toeplitz[2 * pair + half, :, at : at + BLOCK]
                    if i < blocks:
                        tile = tile + closed[i]
                    tiles.append(tile)
                top = functools.reduce(jnp.maximum, tiles)
                top = jnp.max(top, axis=1, keepdims=True)
                tiles = [jnp.exp2(tile - top) for tile in tiles]
                total = jnp.sum(functools.reduce(jnp.add, tiles), axis=1, keepdims=True)
                raw = jnp.concatenate([tile.astype(BF16) for tile in tiles], axis=1)
                mixed = jnp.dot(raw, values, preferred_element_type=F32)
                halves.append(mixed / total)
            gather[1, l, me, rows_of(c), lanes] = jnp.where(low, halves[0], halves[1]).astype(BF16)
        spread(1, l, c)

    def out_project(l, c):
        arrive(1, l, c)
        whole = jnp.concatenate([gather[1, l, j, rows_of(c)] for j in range(tp)], axis=1)
        value = jnp.dot(whole, wbuf[l, 3], preferred_element_type=F32)
        branch[rows_of(c)] = value
        square = jnp.sum(value * value, axis=1, keepdims=True)
        sums[l, c, me] = jnp.broadcast_to(square, (BLOCK, BLOCK)).T[:8]
        for k in range(1, tp):
            sum_copy(l, c, lax.rem(me + k, tp), me).start()

    def finish(l, c):
        for k in range(1, tp):
            peer = lax.rem(me + k, tp)
            sum_copy(l, c, peer, peer).wait_recv()
            sum_copy(l, c, peer, me).wait_send()
        total = functools.reduce(jnp.add, [sums[l, c, j] for j in range(tp)])
        inv = lax.rsqrt(total / width + EPS)
        inv = jnp.broadcast_to(inv[0:1], (BLOCK, BLOCK)).T[:, 0:1]
        gain = gains_ref[l, 1:2, pl.ds(pl.multiple_of(me * cols, 128), cols)]
        new = gather[0, l, me, rows_of(c)].astype(F32) + branch[rows_of(c)] * inv * gain
        new = new.astype(BF16)

        @pl.when(l == layers - 1)
        def _():
            out_ref[rows_of(c)] = new

        @pl.when(l < layers - 1)
        def _():
            later = jnp.minimum(l + 1, layers - 1)
            gather[0, later, me, rows_of(c)] = new
            spread(0, later, c)

    def layer(l, carry):
        for h in range(2 * pairs):
            line = jnp.broadcast_to(bias_ref[l, h : h + 1], (BLOCK, bias_ref.shape[2]))
            skewed = pltpu.roll(line, 0, 1, stride=1, stride_axis=0)
            toeplitz[h, :, :BLOCK] = skewed[:, :BLOCK]
            toeplitz[h, :, BLOCK:] = skewed[:, BLOCK : 2 * BLOCK] + late
        for k in range(3):
            weight_copy(l, k).wait()

        def first(t, carry):
            project(l, chunks - 1 - t)
            return carry

        lax.fori_loop(0, chunks, first, 0)
        weight_copy(l, 3).wait()

        def second(t, carry):
            @pl.when(t < chunks)
            def _():
                attention(l, chunks - 1 - t)

            @pl.when((t >= 1) & (t <= chunks))
            def _():
                out_project(l, chunks - t)

            @pl.when(t >= 2)
            def _():
                finish(l, chunks + 1 - t)

            return carry

        lax.fori_loop(0, chunks + 2, second, 0)
        return carry

    lax.fori_loop(0, layers, layer, 0)


def on_device(tp, sp_count, residual, gains, w_query, w_key, w_value, w_out, rel_bias):
    tokens, cols = residual.shape
    layers, width, _ = w_query.shape
    chunks = tokens // BLOCK
    reach = LEFT * SEG
    heads = cols // HEAD
    far = rel_bias[:, :, 2 * MAXREL :]
    near = (rel_bias[:, :, 1:] - far)[:, :, ::-1] * LOG2E
    line = jnp.concatenate([near, jnp.zeros((layers, heads, BLOCK), F32)], axis=2)
    vmem = pl.BlockSpec(memory_space=pltpu.VMEM)
    hbm = pl.BlockSpec(memory_space=pl.ANY)
    dma = pltpu.SemaphoreType.DMA
    return pl.pallas_call(
        functools.partial(kernel, tp, sp_count),
        out_shape=jax.ShapeDtypeStruct((tokens, cols), BF16),
        in_specs=[vmem, vmem, vmem, hbm, hbm, hbm, hbm],
        out_specs=vmem,
        scratch_shapes=[
            pltpu.VMEM((layers, 4, width, cols), BF16),
            pltpu.VMEM((2, layers, tp, tokens, cols), BF16),
            pltpu.VMEM((layers, reach + tokens, cols), BF16),
            pltpu.VMEM((layers, reach + tokens, cols), BF16),
            pltpu.VMEM((tokens, cols), BF16),
            pltpu.VMEM((tokens, cols), F32),
            pltpu.VMEM((heads, BLOCK, 2 * BLOCK), F32),
            pltpu.VMEM((layers, chunks, tp, 8, BLOCK), F32),
            dma((layers, 4)),
            dma((2, chunks, tp)),
            dma((2, layers, chunks, tp)),
            dma((tp,)),
            dma((chunks, 2)),
            dma((layers, chunks, 2)),
            dma((tp,)),
            dma((layers, chunks, tp)),
        ],
        compiler_params=pltpu.CompilerParams(
            collective_id=0, has_side_effects=True, vmem_limit_bytes=58 * 2**20
        ),
    )(residual, gains, line, w_query, w_key, w_value, w_out)


def solution(mesh):
    return jax.shard_map(
        functools.partial(on_device, mesh.shape["tp"], mesh.shape["sp"]),
        mesh=mesh,
        in_specs=(
            P("sp", "tp"),
            P(),
            P(None, None, "tp"),
            P(None, None, "tp"),
            P(None, None, "tp"),
            P(None, None, "tp"),
            P(None, "tp", None),
        ),
        out_specs=P("sp", "tp"),
        check_vma=False,
    )
```

profile of v0, /device:TPU:9, one launch (start us, length us, event | category | flops | bytes accessed | tf_op | source)
XLA Modules:
  0.0 95.5 jit_solution(14068972438721919060)
XLA Ops:
  0.0 0.8 slice_reduce_fusion
  0.8 0.8 slice_subtract_fusion
  1.6 0.1 rev.3
  1.7 0.6 concatenate.3.bias_ref
  2.4 91.3 %shard_map.73 = bf16[512,512]{1,0:T(8,128)(2,1)} custom-call(bf16[512,512]{1,0:T(8,128)(2,1)} %res_ref.1, f32[2,2,2048]{2,1,0:T(2,128)} %gains_ref.1, f32[2,8,384]{2,1,0:T(8,128)} %concatenate.3.bias_ref, bf16[2,2048,512]{2,1,0:T(8,128)(2,1)} %wq_ref.1, bf16[2,2048,512]{2,1,0:T(8,128)(2,1)} %wk_ref.1, bf16[2,2048,512]{2,1,0:T(8,128)(2,1)} %wv_ref.1, ...), custom_call_target="tpu_custom_call" | custom-call | tf_op jit(solution)/shard_map/pallas_call | solution.py:317
  93.6 1.9 %copy.9 = bf16[512,512]{1,0:T(8,128)(2,1)} copy(bf16[512,512]{1,0:T(8,128)(2,1)} %shard_map.73) | data formatting | bytes 1048576
  (1 shorter events, 0.0 us)
where the time goes:
time: 95.8 us; the launch traced here: 95.5 us
  Pallas kernels  91.3 us (95%)
  local copies, waits for them, and re-layouts  3.42 us (4%)
    pallas_call x1, Pallas kernels, on_device(): pl.pallas_call(functools.partial(kernel, tp, sp_count), out_shape=jax.Sha...  91.3 us

commit v1 on v0

--- a/solution.py
+++ b/solution.py
@@ -107,7 +107,7 @@
     def forward(kind, l, c, source):
         ref = block_of(kind, l, c, source)
         return remote(
-            ref, ref, f_send.at[source], g_recv.at[kind, l, c, source], {"tp": sibling}
+            ref, ref, f_send.at[kind, c, source], g_recv.at[kind, l, c, source], {"tp": sibling}
         )
 
     def spread(kind, l, c):
@@ -115,11 +115,13 @@
             direct(kind, l, c, lax.rem(me + 2 * k, tp), me).start()
         direct(kind, l, c, sibling, me).start()
 
-    def arrive(kind, l, c):
+    def relay(kind, l, c):
         for k in range(1, ychips):
             source = lax.rem(me + 2 * k, tp)
             direct(kind, l, c, source, source).wait_recv()
             forward(kind, l, c, source).start()
+
+    def arrive(kind, l, c):
         direct(kind, l, c, sibling, sibling).wait_recv()
         for k in range(1, ychips):
             source = lax.rem(sibling + 2 * k, tp)
@@ -219,7 +221,7 @@
                         tile = tile + early
                     if i >= blocks - 1:
                         at = (i - blocks + 1) * BLOCK
-                        tile = tile + toeplitz[2 * pair + half, :, at : at + BLOCK]
+                        tile = tile + toeplitz[l, 2 * pair + half, :, at : at + BLOCK]
                     if i < blocks:
                         tile = tile + closed[i]
                     tiles.append(tile)
@@ -265,38 +267,79 @@
             gather[0, later, me, rows_of(c)] = new
             spread(0, later, c)
 
+    def tables(l, carry):
+        far = bias_ref[l, :, 2 * MAXREL :]
+        near = (bias_ref[l, :, : 2 * MAXREL] - far) * LOG2E
+        for h in range(2 * pairs):
+            line = jnp.concatenate([jnp.zeros((1, BLOCK), F32), near[h : h + 1]], axis=1)
+            line = jnp.broadcast_to(line, (2 * BLOCK, 3 * BLOCK))
+            skewed = pltpu.roll(line, 0, 1, stride=1, stride_axis=0)
+            toeplitz[l, h, :, :BLOCK] = skewed[:BLOCK, :BLOCK].T
+            toeplitz[l, h, :, BLOCK:] = skewed[BLOCK:, :BLOCK].T + late
+        return carry
+
+    lax.fori_loop(0, layers, tables, 0)
+
+    for k in range(3):
+        weight_copy(0, k).wait()
+
+    def enter(t, carry):
+        @pl.when(t < chunks)
+        def _():
+            relay(0, 0, chunks - 1 - t)
+
+        @pl.when(t >= 1)
+        def _():
+            project(0, chunks - t)
+
+        return carry
+
+    lax.fori_loop(0, chunks + 1, enter, 0)
+    weight_copy(0, 3).wait()
+
     def layer(l, carry):
-        for h in range(2 * pairs):
-            line = jnp.broadcast_to(bias_ref[l, h : h + 1], (BLOCK, bias_ref.shape[2]))
-            skewed = pltpu.roll(line, 0, 1, stride=1, stride_axis=0)
-            toeplitz[h, :, :BLOCK] = skewed[:, :BLOCK]
-            toeplitz[h, :, BLOCK:] = skewed[:, BLOCK : 2 * BLOCK] + late
-        for k in range(3):
-            weight_copy(l, k).wait()
-
-        def first(t, carry):
-            project(l, chunks - 1 - t)
+        later = jnp.minimum(l + 1, layers - 1)
+        more = l < layers - 1
+
+        def stage(t, lag, needed=True):
+            return (t >= lag) & (t < lag + chunks) & needed
+
+        def step(t, carry):
+            def at(lag):
+                return chunks - 1 - t + lag
+
+            @pl.when(stage(t, 0))
+            def _():
+                attention(l, at(0))
+
+            @pl.when(stage(t, 1))
+            def _():
+                relay(1, l, at(1))
+
+            @pl.when(stage(t, 2))
+            def _():
+                out_project(l, at(2))
+
+            @pl.when(stage(t, 3))
+            def _():
+                finish(l, at(3))
+
+            @pl.when((t == 4) & more)
+            def _():
+                for k in range(4):
+                    weight_copy(later, k).wait()
+
+            @pl.when(stage(t, 4, more))
+            def _():
+                relay(0, later, at(4))
+
+            @pl.when(stage(t, 5, more))
+            def _():
+                project(later, at(5))
+
             return carry
 
-        lax.fori_loop(0, chunks, first, 0)
-        weight_copy(l, 3).wait()
-
-        def second(t, carry):
-            @pl.when(t < chunks)
-            def _():
-                attention(l, chunks - 1 - t)
-
-            @pl.when((t >= 1) & (t <= chunks))
-            def _():
-                out_project(l, chunks - t)
-
-            @pl.when(t >= 2)
-            def _():
-                finish(l, chunks + 1 - t)
-
-            return carry
-
-        lax.fori_loop(0, chunks + 2, second, 0)
+        lax.fori_loop(0, chunks + 5, step, 0)
         return carry
 
     lax.fori_loop(0, layers, layer, 0)
@@ -308,9 +351,6 @@
     chunks = tokens // BLOCK
     reach = LEFT * SEG
     heads = cols // HEAD
-    far = rel_bias[:, :, 2 * MAXREL :]
-    near = (rel_bias[:, :, 1:] - far)[:, :, ::-1] * LOG2E
-    line = jnp.concatenate([near, jnp.zeros((layers, heads, BLOCK), F32)], axis=2)
     vmem = pl.BlockSpec(memory_space=pltpu.VMEM)
     hbm = pl.BlockSpec(memory_space=pl.ANY)
     dma = pltpu.SemaphoreType.DMA
@@ -326,12 +366,12 @@
             pltpu.VMEM((layers, reach + tokens, cols), BF16),
             pltpu.VMEM((tokens, cols), BF16),
             pltpu.VMEM((tokens, cols), F32),
-            pltpu.VMEM((heads, BLOCK, 2 * BLOCK), F32),
+            pltpu.VMEM((layers, heads, BLOCK, 2 * BLOCK), F32),
             pltpu.VMEM((layers, chunks, tp, 8, BLOCK), F32),
             dma((layers, 4)),
             dma((2, chunks, tp)),
             dma((2, layers, chunks, tp)),
-            dma((tp,)),
+            dma((2, chunks, tp)),
             dma((chunks, 2)),
             dma((layers, chunks, 2)),
             dma((tp,)),
@@ -340,7 +380,7 @@
         compiler_params=pltpu.CompilerParams(
             collective_id=0, has_side_effects=True, vmem_limit_bytes=58 * 2**20
         ),
-    )(residual, gains, line, w_query, w_key, w_value, w_out)
+    )(residual, gains, rel_bias, w_query, w_key, w_value, w_out)
 
 
 def solution(mesh):

time: 95.8 us -> 90.9 us (0.949)
  Pallas kernels: 91.3 us -> 88.8 us
  local copies, waits for them, and re-layouts: 3.42 us -> 1.87 us
    pallas_call x1, Pallas kernels: 91.3 us -> 88.8 us  [on_device(): pl.pallas_call(functools.partial(kernel, tp, sp_count), out_shape=jax.Sha...]
where the time goes in v1:
time: 90.9 us; the launch traced here: 90.7 us
  Pallas kernels  88.8 us (98%)
  local copies, waits for them, and re-layouts  1.87 us (2%)
    pallas_call x1, Pallas kernels, on_device(): pl.pallas_call(functools.partial(kernel, tp, sp_count), out_shape=jax.Sha...  88.8 us
    unnamed x1, local copies, waits for them, and re-layouts  1.87 us

profile of v1, /device:TPU:9, one launch (start us, length us, event | category | flops | bytes accessed | tf_op | source)
XLA Modules:
  0.0 90.7 jit_solution(137833266812936910)
XLA Ops:
  0.0 88.8 %shard_map.73 = bf16[512,512]{1,0:T(8,128)(2,1)} custom-call(bf16[512,512]{1,0:T(8,128)(2,1)} %res_ref.1, f32[2,2,2048]{2,1,0:T(2,128)} %gains_ref.1, f32[2,8,257]{2,1,0:T(8,128)} %bias_ref.1, bf16[2,2048,512]{2,1,0:T(8,128)(2,1)} %wq_ref.1, bf16[2,2048,512]{2,1,0:T(8,128)(2,1)} %wk_ref.1, bf16[2,2048,512]{2,1,0:T(8,128)(2,1)} %wv_ref.1, ...), custom_call_target="tpu_custom_call" | custom-call | tf_op jit(solution)/shard_map/pallas_call | solution.py:357
  88.8 1.9 %copy.9 = bf16[512,512]{1,0:T(8,128)(2,1)} copy(bf16[512,512]{1,0:T(8,128)(2,1)} %shard_map.73) | data formatting | bytes 1048576

commit v2 on v1

--- a/solution.py
+++ b/solution.py
@@ -203,6 +203,12 @@
         ]
 
         for pair in range(pairs):
+            if pair == pairs // 2:
+
+                @pl.when(c < chunks - 1)
+                def _():
+                    relay(1, l, jnp.minimum(c + 1, chunks - 1))
+
             lanes = slice(pair * 128, (pair + 1) * 128)
             query = qbuf[rows_of(c), lanes]
             keys = kbuf[l, window, lanes]
@@ -312,34 +318,34 @@
             def _():
                 attention(l, at(0))
 
+            @pl.when(t == chunks)
+            def _():
+                relay(1, l, 0)
+
             @pl.when(stage(t, 1))
             def _():
-                relay(1, l, at(1))
+                out_project(l, at(1))
 
             @pl.when(stage(t, 2))
             def _():
-                out_project(l, at(2))
-
-            @pl.when(stage(t, 3))
-            def _():
-                finish(l, at(3))
-
-            @pl.when((t == 4) & more)
+                finish(l, at(2))
+
+            @pl.when((t == 3) & more)
             def _():
                 for k in range(4):
                     weight_copy(later, k).wait()
 
+            @pl.when(stage(t, 3, more))
+            def _():
+                relay(0, later, at(3))
+
             @pl.when(stage(t, 4, more))
             def _():
-                relay(0, later, at(4))
-
-            @pl.when(stage(t, 5, more))
-            def _():
-                project(later, at(5))
+                project(later, at(4))
 
             return carry
 
-        lax.fori_loop(0, chunks + 5, step, 0)
+        lax.fori_loop(0, chunks + 4, step, 0)
         return carry
 
     lax.fori_loop(0, layers, layer, 0)

time: 90.9 us -> 94.4 us (1.039); the launches traced: 90.7 us -> 93.1 us
  Pallas kernels: 88.8 us -> 91.3 us
    pallas_call x1, Pallas kernels: 88.8 us -> 91.3 us  [on_device(): pl.pallas_call(functools.partial(kernel, tp, sp_count), out_shape=jax.Sha...]
where the time goes in v2:
time: 94.4 us; the launch traced here: 93.1 us
  Pallas kernels  91.3 us (97%)
  local copies, waits for them, and re-layouts  1.87 us (2%)
    pallas_call x1, Pallas kernels, on_device(): pl.pallas_call(functools.partial(kernel, tp, sp_count), out_shape=jax.Sha...  91.3 us

profile of v2, /device:TPU:9, one launch (start us, length us, event | category | flops | bytes accessed | tf_op | source)
XLA Modules:
  0.0 93.1 jit_solution(14572832462305666959)
XLA Ops:
  0.0 91.3 %shard_map.73 = bf16[512,512]{1,0:T(8,128)(2,1)} custom-call(bf16[512,512]{1,0:T(8,128)(2,1)} %res_ref.1, f32[2,2,2048]{2,1,0:T(2,128)} %gains_ref.1, f32[2,8,257]{2,1,0:T(8,128)} %bias_ref.1, bf16[2,2048,512]{2,1,0:T(8,128)(2,1)} %wq_ref.1, bf16[2,2048,512]{2,1,0:T(8,128)(2,1)} %wk_ref.1, bf16[2,2048,512]{2,1,0:T(8,128)(2,1)} %wv_ref.1, ...), custom_call_target="tpu_custom_call" | custom-call | tf_op jit(solution)/shard_map/pallas_call | solution.py:363
  91.3 1.9 %copy.9 = bf16[512,512]{1,0:T(8,128)(2,1)} copy(bf16[512,512]{1,0:T(8,128)(2,1)} %shard_map.73) | data formatting | bytes 1048576
